TPU v7x, 32 devices: a whole 2x2x4 slice. The times are simulated.
32 devices in a mesh: sp: 16 (over z, y, core), tp: 2 (over x).
Axes of the slice: x: 2, y: 2, z: 4, core: 2. Of those that a mesh axis runs over, the one named last changes fastest.
Arguments:
- tokens: bfloat16 [2048, 2048], P(('sp', 'tp')), may hold values from -16 to 16
- w_query: bfloat16 [2048, 1024], P(None, 'tp'), may hold values from -0.110485435 to 0.110485435
- w_key: bfloat16 [2048, 256], P(None, 'tp'), may hold values from -0.15467961 to 0.15467961
- w_value: bfloat16 [2048, 256], P(None, 'tp'), may hold values from -0.125 to 0.125
- cum_gate: float32 [2048, 16], P('sp', 'tp'), may hold values from -371 to 0, as said below
- w_out: bfloat16 [1024, 2048], replicated, may hold values from -0.1875 to 0.1875
Outputs:
- mixed: bfloat16 [2048, 2048], P(('sp', 'tp'))
Inputs may be any that keep to these rules, and one draw needn't show every extreme that they name: `cum_gate`: each head's column does not rise along the positions.
All inputs are finite; a program needn't handle non-finite values.
Results may differ from a plain program's by a relative error of at most 0.012.
Values may be sent and summed in bfloat16 or wider, within the bound.
A program may use at most 64 MiB of HBM per device.

v0:
```python
import math

import jax
import jax.numpy as jnp
from jax import lax
from jax.sharding import PartitionSpec as P

HEAD_DIM = 64


NEG_FILL = -1e30


def shards(tokens, w_query, w_key, w_value, cum_gate, w_out):
    query_cols = w_query.shape[1]
    pair_cols = w_key.shape[1]
    local_heads = query_cols // HEAD_DIM
    local_kv = pair_cols // HEAD_DIM
    group = local_heads // local_kv
    stacked = jnp.concatenate((w_query, w_key, w_value), axis=1)
    joined = jnp.dot(
        lax.all_gather(tokens, "tp", axis=0, tiled=True),
        stacked,
        preferred_element_type=jnp.float32,
    ).astype(jnp.bfloat16)
    row_count = joined.shape[0]
    queries = joined[:, :query_cols].reshape(row_count, local_kv, group, HEAD_DIM)
    keys = joined[:, query_cols : query_cols + pair_cols]
    values = joined[:, query_cols + pair_cols :]
    gate_query = cum_gate.reshape(row_count, local_kv, group)
    gate_every = lax.all_gather(cum_gate, "sp", axis=0, tiled=True)
    keys_every, values_every = (
        lax.all_gather(keys, "sp", axis=0, tiled=True),
        lax.all_gather(values, "sp", axis=0, tiled=True),
    )
    length = keys_every.shape[0]
    width = math.gcd(length, 2048)
    position_shift = lax.axis_index("sp") * row_count
    query_pos = position_shift + jnp.arange(row_count, dtype=jnp.int32)
    last_pos = position_shift + row_count - 1
    scale = HEAD_DIM ** (-0.5)

    def add_block(index, state):
        run_max, run_total, run_acc = state
        block_start = index * width
        key_block = lax.dynamic_slice_in_dim(keys_every, block_start, width, 0)
        value_block = lax.dynamic_slice_in_dim(values_every, block_start, width, 0)
        gate_block = lax.dynamic_slice_in_dim(gate_every, block_start, width, 0)
        gate_key = gate_block.reshape(width, local_kv, group).transpose(1, 2, 0)
        scores = jnp.einsum(
            "tkgd,rkd->tkgr",
            queries,
            key_block.reshape(width, local_kv, HEAD_DIM),
            preferred_element_type=jnp.float32,
        )
        scores = scores * scale + gate_query[..., None] - gate_key[None]
        key_pos = block_start + jnp.arange(width, dtype=jnp.int32)
        allowed = (key_pos[None, :] <= query_pos[:, None])[:, None, None, :]
        scores = jnp.where(allowed, scores, NEG_FILL)
        new_max = jnp.maximum(run_max, jnp.max(scores, axis=-1))
        weights = jnp.where(allowed, jnp.exp(scores - new_max[..., None]), 0.0)
        factor = jnp.exp(run_max - new_max)
        new_total = run_total * factor + jnp.sum(weights, axis=-1)
        gained = jnp.einsum(
            "tkgr,rkd->tkgd",
            weights.astype(jnp.bfloat16),
            value_block.reshape(width, local_kv, HEAD_DIM),
            preferred_element_type=jnp.float32,
        )
        return (new_max, new_total, run_acc * factor[..., None] + gained)

    initial = (
        jnp.full((row_count, local_kv, group), NEG_FILL, jnp.float32),
        jnp.zeros((row_count, local_kv, group), jnp.float32),
        jnp.zeros((row_count, local_kv, group, HEAD_DIM), jnp.float32),
    )
    run_max, run_total, run_acc = lax.fori_loop(0, last_pos // width + 1, add_block, initial)
    attended = (run_acc / run_total[..., None]).astype(jnp.bfloat16).reshape(row_count, query_cols)
    regrouped = lax.all_to_all(attended, "tp", split_axis=0, concat_axis=1, tiled=True)
    return jnp.dot(regrouped, w_out, preferred_element_type=jnp.float32).astype(jnp.bfloat16)


def solution(mesh):
    placed = (
        P(("sp", "tp"), None),
        P(None, "tp"),
        P(None, "tp"),
        P(None, "tp"),
        P("sp", "tp"),
        P(),
    )
    return jax.shard_map(
        shards, mesh=mesh, in_specs=placed, out_specs=P(("sp", "tp"), None), check_vma=False
    )
```

profile of v0, /device:TPU:0, one launch (start us, length us, event | category | flops | bytes accessed | tf_op | source)
XLA Modules:
  0.0 94.7 jit_solution(8654843042355154446)
XLA Ops:
  0.0 0.0 copy-start.1
  0.0 10.3 %all_gather.12 = bf16[128,2048]{1,0:T(8,128)(2,1)S(1)} all-gather(bf16[64,2048]{1,0:T(8,128)(2,1)} %param.8), channel_id=1, replica_groups=mesh['sp'=16,'tp'=2] {'tp'}, dimensions={0}, use_global_device_ids=true | all-gather | bytes 786432 | tf_op jit(solution)/shard_map/all_gather | solution.py:22
  10.3 3.0 %fusion.28 = bf16[128,768]{0,1:T(8,128)(2,1)S(1)} fusion(bf16[128,2048]{1,0:T(8,128)(2,1)S(1)} %all_gather.12, bf16[2048,128]{1,0:T(8,128)(2,1)} %param.11, bf16[2048,128]{1,0:T(8,128)(2,1)} %param.10, bf16[2048,512]{1,0:T(8,128)(2,1)} %param.9), kind=kOutput, calls=%fused_computation.28 | convolution fusion | flops 412188672 | bytes 3866624 | tf_op jit(solution)/shard_map/dot_general | solution.py:21
  13.3 0.0 copy-done.1
  13.3 22.0 %all_gather.14 = f32[2048,8]{0,1:T(8,128)S(1)} all-gather(f32[128,8]{0,1:T(8,128)S(1)} %copy-done.1), channel_id=1, replica_groups=mesh['sp'=16,'tp'=2] {'sp'}, dimensions={0}, use_global_device_ids=true | all-gather | bytes 69632 | tf_op jit(solution)/shard_map/all_gather | solution.py:31
  35.3 0.0 copy-start
  35.4 18.9 %all_gather.15 = bf16[2048,128]{0,1:T(8,128)(2,1)S(1)} all-gather(bf16[128,128]{0,1:T(8,128)(2,1)S(1)} %get-tuple-element.118), channel_id=1, replica_groups=mesh['sp'=16,'tp'=2] {'sp'}, dimensions={0}, use_global_device_ids=true | all-gather | bytes 557056 | tf_op jit(solution)/shard_map/all_gather | solution.py:34
  54.3 20.3 %all_gather.13 = bf16[2048,128]{0,1:T(8,128)(2,1)S(1)} all-gather(bf16[128,128]{0,1:T(8,128)(2,1)S(1)} %get-tuple-element.119), channel_id=1, replica_groups=mesh['sp'=16,'tp'=2] {'sp'}, dimensions={0}, use_global_device_ids=true | all-gather | bytes 557056 | tf_op jit(solution)/shard_map/all_gather | solution.py:33
  74.6 0.0 copy-done
  74.6 9.0 %while.16 = (s32[]{:T(128)}, f32[128,2,4]{0,2,1:T(4,128)S(1)}, f32[128,2,4]{0,2,1:T(4,128)S(1)}, f32[128,2,4,64]{0,3,2,1:T(8,128)S(1)}, s32[]{:T(128)}, /*index=...) while((s32[]{:T(128)}, f32[128,2,4]{0,2,1:T(4,128)S(1)}, ...), condition=%wide.wide.region_3.4_spmd.clone, body=%wide.wide.region_0.3_spmd.clone.sunk | while | flops 577114240 | bytes 28210328 | solution.py:77
  74.6 0.3 broadcast_compare_fusion.3
  75.0 2.6 %fusion.57 = (f32[128,2,4]{0,2,1:T(4,128)S(1)}, f32[2,2048,128,4]{2,1,3,0:T(8,128)S(1)}) fusion(f32[2,4,2048]{2,1,0:T(4,128)S(1)} %bitcast.108, f32[128,2,4]{0,2,1:T(4,128)S(1)} %bitcast.120, pred[128,2048]{0,1:T(8,128)(4,1)S(1)} %broadcast_compare_fusion.3, bf16[2048,2,64,1]{0,2,3,1:T(8,128)(2,1)S(1)} %bitcast.114, ...), kind=kOutput, calls=%fused_computation.7.clone.clone.1 | convolution fusion | flops 278920192 | bytes 9379840 | tf_op jit(solution)/shard_map/while/body/tkgd,rkd->tkgr/dot_general | solution.py:50
  77.6 3.1 %fusion.58 = f32[128,2,4]{0,2,1:T(4,128)S(1)} fusion(f32[2,2048,128,4]{2,1,3,0:T(8,128)S(1)} %get-tuple-element.252, f32[128,2,4]{0,2,1:T(4,128)S(1)} %max.6, f32[2,4,2048]{2,1,0:T(4,128)S(1)} %bitcast.109, f32[128,2,4]{0,2,1:T(4,128)S(1)} %bitcast.121, pred[128,2048]{0,1:T(8,128)(4,1)S(1)} %broadcast_compare_fusion.3), kind=kLoop, calls=%fused_computation.6.clone.clone.1 | loop fusion | flops 14679040 | bytes 8728576 | tf_op jit(solution)/shard_map/while/body/reduce_sum | solution.py:63
  80.8 2.8 %fusion.59 = f32[128,2,4,64]{0,3,2,1:T(8,128)S(1)} fusion(bf16[2048,2,64,1]{0,2,3,1:T(8,128)(2,1)S(1)} %bitcast.113, f32[2,2048,128,4]{2,1,3,0:T(8,128)S(1)} %get-tuple-element.252, f32[128,2,4]{0,2,1:T(4,128)S(1)} %max.6, f32[2,4,2048]{2,1,0:T(4,128)S(1)} %bitcast.110, f32[128,2,4]{0,2,1:T(4,128)S(1)} %bitcast.122, ...), kind=kOutput, calls=%fused_computation.11.clone.clone.1 | convolution fusion | flops 283246592 | bytes 9777152 | tf_op jit(solution)/shard_map/while/body/tkgr,rkd->tkgd/dot_general | solution.py:64
  83.6 0.1 reshape.55
  83.8 0.1 copy.14
  83.9 7.0 %all_to_all.19 = bf16[2,64,512]{2,1,0:T(8,128)(2,1)S(1)} all-to-all(bf16[2,64,512]{2,1,0:T(8,128)(2,1)S(1)} %copy.14), channel_id=1, replica_groups=mesh['sp'=16,'tp'=2] {'tp'}, dimensions={0} | all-to-all | bytes 262144 | tf_op jit(solution)/shard_map/all_to_all | solution.py:79
  91.0 3.7 %convolution_convert_fusion = bf16[64,2048]{1,0:T(8,128)(2,1)} fusion(bf16[64,1024]{1,0:T(8,128)(2,1)S(1)} %bitcast.112, bf16[1024,2048]{1,0:T(8,128)(2,1)} %param.13), kind=kOutput, calls=%fused_computation.26 | convolution fusion | flops 268566528 | bytes 4587520 | tf_op jit(solution)/shard_map/dot_general | solution.py:80
  (13 shorter events, 0.1 us)
Async XLA Ops:
  0.0 13.3 %copy-start.1 = (f32[128,8]{0,1:T(8,128)S(1)}, f32[128,8]{0,1:T(8,128)}, u32[]{:S(2)}) copy-start(f32[128,8]{0,1:T(8,128)} %param.12) | copy-start | bytes 12292
  35.3 39.2 %copy-start = (f32[2048,8]{0,1:T(8,128)}, f32[2048,8]{0,1:T(8,128)S(1)}, u32[]{:S(2)}) copy-start(f32[2048,8]{0,1:T(8,128)S(1)} %all_gather.14) | copy-start | bytes 196612
where the time goes:
time: 94.9 us; the launch traced here: 94.7 us
  blocking collectives  78.5 us (83%)
  matrix products  12.1 us (13%)
  other arithmetic  3.53 us (4%)
    all_gather x1, blocking collectives, shards(): gate_every = lax.all_gather(cum_gate, 'sp', axis=0, tiled=True)  22 us
    all_gather x1, blocking collectives, shards(): lax.all_gather(keys, 'sp', axis=0, tiled=True)  20.3 us
    all_gather x1, blocking collectives, shards(): lax.all_gather(values, 'sp', axis=0, tiled=True)  18.9 us
    all_gather x1, blocking collectives, shards(): lax.all_gather(tokens, 'tp', axis=0, tiled=True)  10.3 us
    all_to_all x1, blocking collectives, shards(): lax.all_to_all(attended, 'tp', split_axis=0, concat_axis=1, tiled=True)  7.03 us
    dot_general x1, matrix products, shards(): jnp.dot(regrouped, w_out, preferred_element_type=jnp.float32)  3.74 us
    reduce_sum x1, other arithmetic, add_block(): new_total = run_total * factor + jnp.sum(weights, axis=-1)  3.13 us
    dot_general x1, matrix products, shards(): jnp.dot(lax.all_gather(tokens, 'tp', axis=0, tiled=True), stacked, prefer...  2.96 us

commit v1 on v0

v1 whole, which is shorter than its diff:
```python
import functools

import jax
import jax.numpy as jnp
from jax import lax
from jax.experimental import pallas as pl
from jax.experimental.pallas import tpu as pltpu
from jax.sharding import PartitionSpec as P

HEAD_DIM = 64
NEG_FILL = -1e30
LANES = 128
GATE_LANES = 32
BF = jnp.bfloat16
F32 = jnp.float32


def split3(x):
    hi = x.astype(BF).astype(F32)
    rest = x - hi
    mid = rest.astype(BF).astype(F32)
    low = (rest - mid).astype(BF).astype(F32)
    return hi, mid, low


def dims(n):
    chips = n // 2
    wide = max(b for b in range(1, chips + 1) if chips % b == 0 and b * b <= chips)
    return chips // wide, wide


def kernel(
    n,
    parts,
    tok_hbm,
    wq_hbm,
    wk_hbm,
    wv_hbm,
    gate_hbm,
    wo_hbm,
    out_ref,
    tok,
    wq,
    wk,
    wv,
    wo,
    gate,
    qrows,
    kv,
    gates,
    qg,
    run_max,
    run_sum,
    acc,
    att,
    att_in,
    load_sem,
    tok_send,
    tok_recv,
    att_send,
    att_recv,
    z_send,
    y_send,
    c_send,
    recv,
):
    deep, wide = dims(n)
    me = lax.axis_index("sp")
    tp = lax.axis_index("tp")
    core = lax.rem(me, 2)
    y = lax.rem(me // 2, wide)
    z = me // (2 * wide)
    rows = tok_hbm.shape[0]
    block = rows * parts
    heads = gate_hbm.shape[1]
    pc = wk_hbm.shape[1]
    local_kv = pc // HEAD_DIM
    group = heads // local_kv
    qc = heads * HEAD_DIM
    kw = pc if pc % LANES == 0 else 2 * pc
    cols = heads * block

    def index(zz, yy, cc):
        return (zz * wide + yy) * 2 + cc

    def peer(j):
        return lax.rem(tp + j, parts)

    loads = [
        pltpu.make_async_copy(src, dst, load_sem.at[i])
        for i, (src, dst) in enumerate(
            (
                (tok_hbm, tok.at[0]),
                (gate_hbm, gate),
                (wk_hbm, wk),
                (wv_hbm, wv),
                (wq_hbm, wq),
                (wo_hbm, wo),
            )
        )
    ]
    for load in loads:
        load.start()

    barrier = pltpu.get_barrier_semaphore()
    for j in range(1, parts):
        pl.semaphore_signal(barrier, inc=1, device_id={"tp": peer(j)})
    for j in range(1, deep):
        pl.semaphore_signal(barrier, inc=1, device_id={"sp": index(lax.rem(z + j, deep), y, core)})
    for j in range(1, wide):
        pl.semaphore_signal(barrier, inc=1, device_id={"sp": index(z, lax.rem(y + j, wide), core)})
    pl.semaphore_signal(barrier, inc=1, device_id={"sp": index(z, y, 1 - core)})
    loads[0].wait()
    loads[1].wait()

    turned = jnp.concatenate(
        [gate[pl.ds(pl.multiple_of(peer(j) * rows, rows), rows), :] for j in range(parts)], axis=0
    )
    hi, mid, low = split3(turned)
    fill = GATE_LANES - 3 * heads
    per_token = jnp.concatenate((hi, mid, low, jnp.ones((block, fill), F32)), axis=1)
    pack = LANES // GATE_LANES
    span = block // pack
    gates[me] = jnp.concatenate(
        [per_token[j * span : (j + 1) * span, :] for j in range(pack)], axis=1
    ).astype(BF)

    pl.semaphore_wait(barrier, parts - 1 + deep - 1 + wide - 1 + 1)

    tok_copies = []
    for j in range(1, parts):
        copy = pltpu.make_async_remote_copy(
            src_ref=tok.at[0],
            dst_ref=tok.at[parts - j],
            send_sem=tok_send.at[j],
            recv_sem=tok_recv.at[parts - j],
            device_id={"tp": peer(j)},
        )
        copy.start()
        tok_copies.append(copy)

    def view(item, who):
        if item == 0:
            return gates.at[who]
        if item == 1:
            return kv.at[who, pl.ds(0, rows)]
        return kv.at[who, pl.ds(rows, block - rows)]

    def push(item, who, send_sem, target):
        return pltpu.make_async_remote_copy(
            src_ref=view(item, who),
            dst_ref=view(item, who),
            send_sem=send_sem,
            recv_sem=recv.at[item, who],
            device_id={"sp": target},
        )

    def arrived(item, who):
        push(item, who, z_send.at[item, 0], me).wait_recv()

    def z_push(item, zz):
        return push(item, me, z_send.at[item, zz], index(zz, y, core))

    def y_push(item, zz, yy):
        return push(item, index(zz, y, core), y_send.at[item, zz, yy], index(z, yy, core))

    def c_push(item, zz, yy):
        return push(item, index(zz, yy, core), c_send.at[item, zz, yy], index(z, y, 1 - core))

    def loop(lo, hi, body):
        def step(i, carry):
            body(i)
            return carry

        lax.fori_loop(lo, hi, step, 0)

    def stage_own(item):
        loop(z + 1, deep, lambda zz: z_push(item, zz).start())
        loop(y + 1, wide, lambda yy: y_push(item, z, yy).start())

        @pl.when(core == 0)
        def _():
            c_push(item, z, y).start()

    def other_y(fn):
        loop(0, y, fn)
        loop(y + 1, wide, fn)

    def stage_z(item):
        def one(zz):
            arrived(item, index(zz, y, core))
            other_y(lambda yy: y_push(item, zz, yy).start())
            c_push(item, zz, y).start()

        loop(0, z, one)

    def stage_y(item):
        def at(zz, yy):
            arrived(item, index(zz, yy, core))
            c_push(item, zz, yy).start()

        loop(0, z, lambda zz: other_y(lambda yy: at(zz, yy)))
        loop(0, y, lambda yy: at(z, yy))

    def stage_c(item):
        def at(zz, yy):
            arrived(item, index(zz, yy, 1 - core))

        loop(0, z, lambda zz: loop(0, wide, lambda yy: at(zz, yy)))
        loop(0, y, lambda yy: at(z, yy))

        @pl.when(core == 1)
        def _():
            at(z, y)

    def drain(item):
        loop(z + 1, deep, lambda zz: z_push(item, zz).wait_send())
        loop(y + 1, wide, lambda yy: y_push(item, z, yy).wait_send())

        @pl.when(core == 0)
        def _():
            c_push(item, z, y).wait_send()

        def one(zz):
            other_y(lambda yy: y_push(item, zz, yy).wait_send())
            loop(0, wide, lambda yy: c_push(item, zz, yy).wait_send())

        loop(0, z, one)
        loop(0, y, lambda yy: c_push(item, z, yy).wait_send())

    stage_own(0)

    def project(j, with_kv):
        x = tok[j]
        if with_kv:
            key = jnp.dot(x, wk[...], preferred_element_type=F32)
            value = jnp.dot(x, wv[...], preferred_element_type=F32)
            kv[me, j * rows : (j + 1) * rows, :] = jnp.concatenate((key, value), axis=1).astype(BF)
        else:
            qrows[j * rows : (j + 1) * rows, :] = jnp.dot(
                x, wq[...], preferred_element_type=F32
            ).astype(BF)

    loads[2].wait()
    loads[3].wait()
    project(0, True)
    stage_own(1)
    loads[4].wait()
    project(0, False)
    stage_z(0)
    stage_z(1)
    stage_y(0)
    stage_y(1)
    for j in range(1, parts):
        tok_copies[parts - j - 1].wait_recv()
        project(j, True)
    stage_own(2)
    for j in range(1, parts):
        project(j, False)

    scale = HEAD_DIM ** (-0.5)
    lane = lax.broadcasted_iota(jnp.int32, (block, LANES), 1)
    query = qrows[...].astype(F32) * scale
    for h in range(heads):
        g = h // group
        place = []
        if g > 0:
            place.append(jnp.zeros((block, g * HEAD_DIM), F32))
        place.append(query[:, h * HEAD_DIM : (h + 1) * HEAD_DIM])
        if kw - (g + 1) * HEAD_DIM > 0:
            place.append(jnp.zeros((block, kw - (g + 1) * HEAD_DIM), F32))
        at_gate = (lane == h) | (lane == heads + h) | (lane == 2 * heads + h)
        side = jnp.where(at_gate, -1.0, 0.0)
        for i, piece in enumerate((hi, mid, low)):
            side = jnp.where(lane == 3 * heads + i, piece[:, h : h + 1], side)
        both = jnp.concatenate(place + [side], axis=1)
        qg[:, h * block : (h + 1) * block] = both.T.astype(BF)

    stage_c(0)
    stage_c(1)

    def unpack_gates(who):
        packed = gates[who].astype(F32)
        out = [packed] + [
            pltpu.roll(packed, LANES - j * GATE_LANES, 1) for j in range(1, pack)
        ]
        return jnp.concatenate(out, axis=0).astype(BF)

    def attend(first, count, lo, size, diagonal):
        width = count * size
        for_keys, for_gates = [], []
        for i in range(count):
            for_keys.append(kv[first + i, lo : lo + size, :])
            for_gates.append(unpack_gates(first + i)[lo : lo + size, :])
        keyval = jnp.concatenate(for_keys, axis=0) if count > 1 else for_keys[0]
        gate_part = jnp.concatenate(for_gates, axis=0) if count > 1 else for_gates[0]
        left = jnp.concatenate((keyval[:, :kw], gate_part), axis=1)
        value_t = keyval[:, pc:].astype(F32).T.astype(BF)
        for g in range(local_kv):
            at = slice(g * group * block, (g + 1) * group * block)
            scores = jnp.dot(left, qg[:, at], preferred_element_type=F32)
            if diagonal:
                turn = tp * rows
                key_pos = lax.rem(
                    lax.broadcasted_iota(jnp.int32, (width, block), 0) + turn, block
                )
                query_pos = lax.rem(
                    lax.broadcasted_iota(jnp.int32, (width, block), 1) + turn, block
                )
                allowed = jnp.concatenate([jnp.where(key_pos <= query_pos, 1.0, 0.0)] * group, axis=1) > 0.5
                scores = jnp.where(allowed, scores, NEG_FILL)
                new_max = jnp.max(scores, axis=0, keepdims=True)
            else:
                old_max = run_max[:, at]
                new_max = jnp.maximum(old_max, jnp.max(scores, axis=0, keepdims=True))
            weights = jnp.exp(scores - new_max)
            if diagonal:
                weights = jnp.where(allowed, weights, 0.0)
            total = jnp.sum(weights, axis=0, keepdims=True)
            gained = jnp.dot(
                value_t[g * HEAD_DIM : (g + 1) * HEAD_DIM, :],
                weights.astype(BF),
                preferred_element_type=F32,
            )
            if diagonal:
                run_sum[:, at] = total
                acc[:, at] = gained
            else:
                factor = jnp.exp(old_max - new_max)
                run_sum[:, at] = run_sum[:, at] * factor + total
                acc[:, at] = acc[:, at] * factor + gained
            run_max[:, at] = new_max

    def bits(limit):
        out = []
        size = 1
        while size < limit and size < 8:
            out.append(size)
            size *= 2
        return out[::-1]

    big = 8

    def big_part(lo, size):
        loop(0, me // big, lambda i: attend(i * big, big, lo, size, False))

    def small_part(lo, size):
        for count in bits(n):
            @pl.when(lax.rem(me // count, 2) == 1)
            def _():
                attend(me // (2 * count) * (2 * count), count, lo, size, False)

    attend(me, 1, 0, block, True)
    big_part(0, rows)
    stage_z(2)
    small_part(0, rows)
    stage_y(2)
    stage_c(2)
    big_part(rows, block - rows)
    small_part(rows, block - rows)

    done = acc[...] / run_sum[...]
    stacked = jnp.concatenate([done[:, h * block : (h + 1) * block] for h in range(heads)], axis=0)
    att[...] = stacked.T.astype(BF).reshape(parts, rows, qc)
    att_copies = []
    for j in range(1, parts):
        copy = pltpu.make_async_remote_copy(
            src_ref=att.at[j],
            dst_ref=att_in.at[parts - j],
            send_sem=att_send.at[j],
            recv_sem=att_recv.at[parts - j],
            device_id={"tp": peer(j)},
        )
        copy.start()
        att_copies.append(copy)
    loads[5].wait()

    def w_rows(j):
        return wo[pl.ds(pl.multiple_of(peer(j) * qc, qc), qc), :]

    mixed = jnp.dot(att[0], w_rows(0), preferred_element_type=F32)
    for j in range(1, parts):
        att_copies[parts - j - 1].wait_recv()
        mixed = mixed + jnp.dot(att_in[j], w_rows(j), preferred_element_type=F32)
    out_ref[...] = mixed.astype(BF)

    for copy in tok_copies + att_copies:
        copy.wait_send()
    for item in range(3):
        drain(item)


def shards(n, parts, tokens, w_query, w_key, w_value, cum_gate, w_out):
    deep, wide = dims(n)
    rows, width = tokens.shape
    block = rows * parts
    heads = cum_gate.shape[1]
    pc = w_key.shape[1]
    qc = w_query.shape[1]
    kw = pc if pc % LANES == 0 else 2 * pc
    cols = heads * block
    span = block * GATE_LANES // LANES
    dma = pltpu.SemaphoreType.DMA
    return pl.pallas_call(
        functools.partial(kernel, n, parts),
        out_shape=jax.ShapeDtypeStruct((rows, w_out.shape[1]), BF),
        in_specs=[pl.BlockSpec(memory_space=pl.ANY)] * 6,
        out_specs=pl.BlockSpec(memory_space=pltpu.VMEM),
        scratch_shapes=[
            pltpu.VMEM((parts, rows, width), BF),
            pltpu.VMEM(w_query.shape, BF),
            pltpu.VMEM(w_key.shape, BF),
            pltpu.VMEM(w_value.shape, BF),
            pltpu.VMEM(w_out.shape, BF),
            pltpu.VMEM(cum_gate.shape, F32),
            pltpu.VMEM((block, qc), BF),
            pltpu.VMEM((n, block, 2 * pc), BF),
            pltpu.VMEM((n, span, LANES), BF),
            pltpu.VMEM((kw + LANES, cols), BF),
            pltpu.VMEM((1, cols), F32),
            pltpu.VMEM((1, cols), F32),
            pltpu.VMEM((HEAD_DIM, cols), F32),
            pltpu.VMEM((parts, rows, qc), BF),
            pltpu.VMEM((parts, rows, qc), BF),
            dma((6,)),
            dma((parts,)),
            dma((parts,)),
            dma((parts,)),
            dma((parts,)),
            dma((3, deep)),
            dma((3, deep, wide)),
            dma((3, deep, wide)),
            dma((3, n)),
        ],
        compiler_params=pltpu.CompilerParams(
            collective_id=0, has_side_effects=True, vmem_limit_bytes=48 * 1024 * 1024
        ),
    )(tokens, w_query, w_key, w_value, cum_gate, w_out)


def solution(mesh):
    n, parts = mesh.shape["sp"], mesh.shape["tp"]
    placed = (
        P(("sp", "tp"), None),
        P(None, "tp"),
        P(None, "tp"),
        P(None, "tp"),
        P("sp", "tp"),
        P(),
    )
    return jax.shard_map(
        functools.partial(shards, n, parts),
        mesh=mesh,
        in_specs=placed,
        out_specs=P(("sp", "tp"), None),
        check_vma=False,
    )
```

time: 94.9 us -> 34.4 us (0.36)
  the two profiles are of different devices: /device:TPU:0 before, /device:TPU:29 now
where the time goes in v1:
time: 34.4 us; the launch traced here: 34.1 us
  Pallas kernels  28 us (81%)
  local copies, waits for them, and re-layouts  6.11 us (18%)
    pallas_call x1, Pallas kernels, shards(): pl.pallas_call(functools.partial(kernel, n, parts), out_shape=jax.ShapeDt...  28 us
    unnamed x10, local copies, waits for them, and re-layouts  6.11 us

profile of v1, /device:TPU:29, one launch (start us, length us, event | category | flops | bytes accessed | tf_op | source)
XLA Modules:
  0.0 34.1 jit_solution(10422296113260588384)
XLA Ops:
  0.0 0.8 %copy.7.gate_hbm = f32[128,8]{1,0:T(8,128)S(1)} copy(f32[128,8]{0,1:T(8,128)} %param.10) | data formatting | bytes 8192 | tf_op args[4]
  0.8 0.0 copy-start
  0.8 1.6 %copy-done = bf16[2048,512]{1,0:T(8,128)(2,1)S(1)} copy-done((bf16[2048,512]{1,0:T(8,128)(2,1)S(1)}, bf16[2048,512]{1,0:T(8,128)(2,1)}, u32[]{:S(2)}) %copy-start) | copy-done | bytes 2097176
  2.4 0.0 copy-start.1
  2.4 1.0 %copy-done.1 = bf16[2048,128]{1,0:T(8,128)(2,1)S(1)} copy-done((bf16[2048,128]{1,0:T(8,128)(2,1)S(1)}, bf16[2048,128]{1,0:T(8,128)(2,1)}, u32[]{:S(2)}) %copy-start.1) | copy-done | bytes 524312
  3.4 0.0 copy-start.2
  3.4 1.0 %copy-done.2 = bf16[2048,128]{1,0:T(8,128)(2,1)S(1)} copy-done((bf16[2048,128]{1,0:T(8,128)(2,1)S(1)}, bf16[2048,128]{1,0:T(8,128)(2,1)}, u32[]{:S(2)}) %copy-start.2) | copy-done | bytes 524312
  4.5 0.0 copy-start.3
  4.5 0.9 %copy-done.3 = bf16[64,2048]{1,0:T(8,128)(2,1)S(1)} copy-done((bf16[64,2048]{1,0:T(8,128)(2,1)S(1)}, bf16[64,2048]{1,0:T(8,128)(2,1)}, u32[]{:S(2)}) %copy-start.3) | copy-done | bytes 262168
  5.4 28.0 %shard_map.64 = bf16[64,2048]{1,0:T(8,128)(2,1)S(1)} custom-call(bf16[64,2048]{1,0:T(8,128)(2,1)S(1)} %copy-done.3, bf16[2048,512]{1,0:T(8,128)(2,1)S(1)} %copy-done, bf16[2048,128]{1,0:T(8,128)(2,1)S(1)} %copy-done.1, bf16[2048,128]{1,0:T(8,128)(2,1)S(1)} %copy-done.2, f32[128,8]{1,0:T(8,128)S(1)} %copy.7.gate_hbm, bf16[1024,2048]{1,0:T(8,128)(2,1)} %wo_hbm.1), custom_call_target="tpu_custom_call" | custom-call | tf_op jit(solution)/shard_map/pallas_call | solution.py:404
  33.4 0.7 %copy.9 = bf16[64,2048]{1,0:T(8,128)(2,1)} copy(bf16[64,2048]{1,0:T(8,128)(2,1)S(1)} %shard_map.64) | data formatting | bytes 524288
Async XLA Ops:
  0.8 1.6 %copy-start = (bf16[2048,512]{1,0:T(8,128)(2,1)S(1)}, bf16[2048,512]{1,0:T(8,128)(2,1)}, u32[]{:S(2)}) copy-start(bf16[2048,512]{1,0:T(8,128)(2,1)} %wq_hbm.1) | copy-start | bytes 6291460
  2.4 1.0 %copy-start.1 = (bf16[2048,128]{1,0:T(8,128)(2,1)S(1)}, bf16[2048,128]{1,0:T(8,128)(2,1)}, u32[]{:S(2)}) copy-start(bf16[2048,128]{1,0:T(8,128)(2,1)} %wk_hbm.1) | copy-start | bytes 1572868
  3.4 1.0 %copy-start.2 = (bf16[2048,128]{1,0:T(8,128)(2,1)S(1)}, bf16[2048,128]{1,0:T(8,128)(2,1)}, u32[]{:S(2)}) copy-start(bf16[2048,128]{1,0:T(8,128)(2,1)} %wv_hbm.1) | copy-start | bytes 1572868
  4.5 0.9 %copy-start.3 = (bf16[64,2048]{1,0:T(8,128)(2,1)S(1)}, bf16[64,2048]{1,0:T(8,128)(2,1)}, u32[]{:S(2)}) copy-start(bf16[64,2048]{1,0:T(8,128)(2,1)} %tok_hbm.1) | copy-start | bytes 786436

commit v2 on v1

v2 whole, which is shorter than its diff:
```python
import functools
import math

import jax
import jax.numpy as jnp
from jax import lax
from jax.experimental import pallas as pl
from jax.experimental.pallas import tpu as pltpu
from jax.sharding import PartitionSpec as P

HEAD_DIM = 64
NEG_FILL = -1e30
LANES = 128
GATE_LANES = 32
VMEM_LIMIT = 67_043_328
BF = jnp.bfloat16
F32 = jnp.float32


def split3(x):
    hi = x.astype(BF).astype(F32)
    rest = x - hi
    mid = rest.astype(BF).astype(F32)
    low = (rest - mid).astype(BF).astype(F32)
    return hi, mid, low


def dims(n):
    chips = n // 2
    wide = max(b for b in range(1, chips + 1) if chips % b == 0 and b * b <= chips)
    return chips // wide, wide


def chunk_count(parts):
    return 1


def kernel(
    n,
    parts,
    tok_hbm,
    wq_hbm,
    wk_hbm,
    wv_hbm,
    gate_hbm,
    wo_hbm,
    out_ref,
    tok,
    wq,
    wkv,
    wo,
    gate_t,
    gate,
    qrows,
    kv,
    gates,
    sides,
    qg,
    run_max,
    run_sum,
    acc,
    att,
    att_in,
    load_sem,
    tok_send,
    tok_recv,
    att_send,
    att_recv,
    z_send,
    y_send,
    c_send,
    recv,
):
    deep, wide = dims(n)
    me = lax.axis_index("sp")
    tp = lax.axis_index("tp")
    core = lax.rem(me, 2)
    y = lax.rem(me // 2, wide)
    z = me // (2 * wide)
    rows = tok_hbm.shape[0]
    block = rows * parts
    heads = gate_hbm.shape[0]
    pc = wk_hbm.shape[1]
    local_kv = pc // HEAD_DIM
    group = heads // local_kv
    qc = heads * HEAD_DIM
    kw = pc if pc % LANES == 0 else 2 * pc
    joined = pc % LANES == 0
    pieces = chunk_count(parts)
    part = rows // pieces
    items = 2 + (parts - 1) * pieces

    def index(zz, yy, cc):
        return (zz * wide + yy) * 2 + cc

    half = n // 2
    mine = z * wide + y

    def slot(zz, yy, cc):
        return cc * half + zz * wide + yy

    own = slot(z, y, core)

    def peer(j):
        return lax.rem(tp + j, parts)

    loads = [
        pltpu.make_async_copy(src, dst, load_sem.at[i])
        for i, (src, dst) in enumerate(
            (
                (tok_hbm, tok.at[0]),
                (gate_hbm, gate_t),
                (wk_hbm, wkv.at[:, pl.ds(0, pc)] if joined else wkv.at[0]),
                (wv_hbm, wkv.at[:, pl.ds(pc, pc)] if joined else wkv.at[1]),
                (wq_hbm, wq),
                (wo_hbm, wo),
            )
        )
    ]
    for load in loads:
        load.start()

    kv[...] = jnp.zeros_like(kv)

    barrier = pltpu.get_barrier_semaphore()
    for j in range(1, parts):
        pl.semaphore_signal(barrier, inc=1, device_id={"tp": peer(j)})
    for j in range(1, deep):
        pl.semaphore_signal(barrier, inc=1, device_id={"sp": index(lax.rem(z + j, deep), y, core)})
    for j in range(1, wide):
        pl.semaphore_signal(barrier, inc=1, device_id={"sp": index(z, lax.rem(y + j, wide), core)})
    pl.semaphore_signal(barrier, inc=1, device_id={"sp": index(z, y, 1 - core)})
    loads[0].wait()
    loads[1].wait()

    gate[...] = gate_t[...].T
    turned = jnp.concatenate(
        [gate[pl.ds(pl.multiple_of(peer(j) * rows, rows), rows), :] for j in range(parts)], axis=0
    )
    hi, mid, low = split3(turned)
    fill = GATE_LANES - 3 * heads
    per_token = jnp.concatenate((hi, mid, low, jnp.ones((block, fill), F32)), axis=1)
    pack = LANES // GATE_LANES
    span = block // pack
    gates[own] = jnp.concatenate(
        [per_token[j * span : (j + 1) * span, :] for j in range(pack)], axis=1
    ).astype(BF)

    pl.semaphore_wait(barrier, parts - 1 + deep - 1 + wide - 1 + 1)

    tok_copies = {}
    for j in range(1, parts):
        for q in range(pieces):
            at = pl.ds(q * part, part)
            copy = pltpu.make_async_remote_copy(
                src_ref=tok.at[0, at],
                dst_ref=tok.at[parts - j, at],
                send_sem=tok_send.at[j, q],
                recv_sem=tok_recv.at[parts - j, q],
                device_id={"tp": peer(j)},
            )
            copy.start()
            tok_copies[j, q] = copy

    def view(item, who):
        if item == 0:
            return gates.at[who]
        if item == 1:
            return kv.at[who, pl.ds(0, rows)]
        return kv.at[who, pl.ds(rows + (item - 2) * part, part)]

    def push(item, who, send_sem, target):
        return pltpu.make_async_remote_copy(
            src_ref=view(item, who),
            dst_ref=view(item, who),
            send_sem=send_sem,
            recv_sem=recv.at[item, who],
            device_id={"sp": target},
        )

    def arrived(item, who):
        push(item, who, z_send.at[item, 0], me).wait_recv()

    def z_push(item, zz):
        return push(item, own, z_send.at[item, zz], index(zz, y, core))

    def y_push(item, zz, yy):
        return push(item, slot(zz, y, core), y_send.at[item, zz, yy], index(z, yy, core))

    def c_push(item, zz, yy):
        return push(item, slot(zz, yy, core), c_send.at[item, zz, yy], index(z, y, 1 - core))

    def loop(lo, hi, body):
        def step(i, carry):
            body(i)
            return carry

        lax.fori_loop(lo, hi, step, 0)

    def stage_own(item):
        loop(z + 1, deep, lambda zz: z_push(item, deep + z - zz).start())
        loop(y + 1, wide, lambda yy: y_push(item, z, yy).start())

        @pl.when(core == 0)
        def _():
            c_push(item, z, y).start()

    def other_y(fn):
        loop(0, y, fn)
        loop(y + 1, wide, fn)

    def stage_z(item):
        def one(zz):
            arrived(item, slot(zz, y, core))
            other_y(lambda yy: y_push(item, zz, yy).start())
            c_push(item, zz, y).start()

        loop(0, z, one)

    def stage_y(item):
        def at(zz, yy):
            arrived(item, slot(zz, yy, core))
            c_push(item, zz, yy).start()

        loop(0, z, lambda zz: other_y(lambda yy: at(zz, yy)))
        loop(0, y, lambda yy: at(z, yy))

    def stage_c(item):
        def at(zz, yy):
            arrived(item, slot(zz, yy, 1 - core))

        loop(0, z, lambda zz: loop(0, wide, lambda yy: at(zz, yy)))
        loop(0, y, lambda yy: at(z, yy))

        @pl.when(core == 1)
        def _():
            at(z, y)

    def drain(item):
        loop(z + 1, deep, lambda zz: z_push(item, zz).wait_send())
        loop(y + 1, wide, lambda yy: y_push(item, z, yy).wait_send())

        @pl.when(core == 0)
        def _():
            c_push(item, z, y).wait_send()

        def one(zz):
            other_y(lambda yy: y_push(item, zz, yy).wait_send())
            loop(0, wide, lambda yy: c_push(item, zz, yy).wait_send())

        loop(0, z, one)
        loop(0, y, lambda yy: c_push(item, z, yy).wait_send())

    stage_own(0)

    def project_kv(j, lo, size):
        x = tok[j, lo : lo + size, :]
        if joined:
            both = jnp.dot(x, wkv[...], preferred_element_type=F32)
        else:
            both = jnp.concatenate(
                [jnp.dot(x, wkv[i], preferred_element_type=F32) for i in range(2)], axis=1
            )
        kv[own, j * rows + lo : j * rows + lo + size, :] = both.astype(BF)

    def project_q(j):
        qrows[j * rows : (j + 1) * rows, :] = jnp.dot(
            tok[j], wq[...], preferred_element_type=F32
        ).astype(BF)

    loads[2].wait()
    loads[3].wait()
    project_kv(0, 0, rows)
    stage_own(1)
    loads[4].wait()
    project_q(0)
    stage_z(0)
    stage_z(1)
    stage_y(0)
    stage_y(1)
    for item in range(2, items):
        j, q = 1 + (item - 2) // pieces, (item - 2) % pieces
        tok_copies[parts - j, q].wait_recv()
        project_kv(j, q * part, part)
        stage_own(item)
    for j in range(1, parts):
        project_q(j)

    scale = HEAD_DIM ** (-0.5)
    lane = lax.broadcasted_iota(jnp.int32, (block, LANES), 1)
    query = qrows[...].astype(F32) * scale
    for h in range(heads):
        g = h // group
        place = []
        if g > 0:
            place.append(jnp.zeros((block, g * HEAD_DIM), F32))
        place.append(query[:, h * HEAD_DIM : (h + 1) * HEAD_DIM])
        if kw - (g + 1) * HEAD_DIM > 0:
            place.append(jnp.zeros((block, kw - (g + 1) * HEAD_DIM), F32))
        at_gate = (lane == h) | (lane == heads + h) | (lane == 2 * heads + h)
        side = jnp.where(at_gate, -1.0, 0.0)
        for i, piece in enumerate((hi, mid, low)):
            side = jnp.where(lane == 3 * heads + i, piece[:, h : h + 1], side)
        both = jnp.concatenate(place + [side], axis=1)
        qg[:, h * block : (h + 1) * block] = both.T.astype(BF)

    def unpack_gates(who):
        packed = gates[who].astype(F32)
        out = [packed] + [
            pltpu.roll(packed, LANES - j * GATE_LANES, 1) for j in range(1, pack)
        ]
        sides[who] = jnp.concatenate(out, axis=0).astype(BF)

    sides[...] = jnp.zeros_like(sides)
    loop(core * half, core * half + mine + 1, unpack_gates)
    big = math.gcd(8, half)
    steps = mine // big
    every = tuple(range(local_kv))

    def attend(cc, step, lo, size, last):
        first = cc * half + step * big
        width = big * size
        keyval = kv[pl.ds(first, big), lo : lo + size, :].reshape(width, 2 * pc)
        gate_part = sides[pl.ds(first, big), lo : lo + size, :].reshape(width, LANES)
        left = jnp.concatenate((keyval[:, :kw], gate_part), axis=1)
        value_t = keyval[:, pc:].astype(F32).T.astype(BF)
        if last:
            row = lax.broadcasted_iota(jnp.int32, (width, block), 0)
            which = 2 * (step * big + row // size) + cc
            key_at = lax.rem(lo + lax.rem(row, size) + tp * rows, block)
            query_at = lax.rem(lax.broadcasted_iota(jnp.int32, (width, block), 1) + tp * rows, block)
            key_pos, query_pos = which * block + key_at, me * block + query_at
            bias = jnp.where(key_pos <= query_pos, 0.0, NEG_FILL)
            bias = jnp.concatenate([bias] * group, axis=1)
        for g in every:
            at = slice(g * group * block, (g + 1) * group * block)
            scores = jnp.dot(left, qg[:, at], preferred_element_type=F32)
            if last:
                scores = scores + bias
            old_max = run_max[:, at]
            new_max = jnp.maximum(old_max, jnp.max(scores, axis=0, keepdims=True))
            weights = jnp.exp(scores - new_max)
            total = jnp.sum(weights, axis=0, keepdims=True)
            gained = jnp.dot(
                value_t[g * HEAD_DIM : (g + 1) * HEAD_DIM, :],
                weights.astype(BF),
                preferred_element_type=F32,
            )
            factor = jnp.exp(old_max - new_max)
            run_sum[:, at] = run_sum[:, at] * factor + total
            acc[:, at] = acc[:, at] * factor + gained
            run_max[:, at] = new_max

    run_max[...] = jnp.full_like(run_max, NEG_FILL)
    run_sum[...] = jnp.zeros_like(run_sum)
    acc[...] = jnp.zeros_like(acc)
    def attend_all(cc, lo, size):
        loop(0, steps, lambda i: attend(cc, i, lo, size, False))
        attend(cc, steps, lo, size, True)

    for item in range(2, items):
        stage_z(item)
    attend_all(core, 0, rows)
    stage_c(0)
    stage_c(1)
    loop((1 - core) * half, (1 - core) * half + mine + core, unpack_gates)
    attend_all(1 - core, 0, rows)
    for item in range(2, items):
        stage_y(item)
    attend_all(core, rows, block - rows)
    for item in range(2, items):
        stage_c(item)
    attend_all(1 - core, rows, block - rows)

    att_copies = []
    gc = qc // local_kv
    for g in every:
        at = slice(g * group * block, (g + 1) * group * block)
        done = acc[:, at] / run_sum[:, at]
        stacked = jnp.concatenate(
            [done[:, h * block : (h + 1) * block] for h in range(group)], axis=0
        )
        att[g] = stacked.T.astype(BF).reshape(parts, rows, gc)
        for j in range(1, parts):
            copy = pltpu.make_async_remote_copy(
                src_ref=att.at[g, j],
                dst_ref=att_in.at[g, parts - j],
                send_sem=att_send.at[g, j],
                recv_sem=att_recv.at[g, parts - j],
                device_id={"tp": peer(j)},
            )
            copy.start()
            att_copies.append(copy)
    loads[5].wait()

    def w_rows(g, j):
        return wo[pl.ds(pl.multiple_of(peer(j) * qc + g * gc, gc), gc), :]

    mixed = None
    for g in every:
        term = jnp.dot(att[g, 0], w_rows(g, 0), preferred_element_type=F32)
        mixed = term if mixed is None else mixed + term
    for g in every:
        for j in range(1, parts):
            att_copies[g * (parts - 1) + parts - j - 1].wait_recv()
            mixed = mixed + jnp.dot(att_in[g, j], w_rows(g, j), preferred_element_type=F32)
    out_ref[...] = mixed.astype(BF)

    for copy in list(tok_copies.values()) + att_copies:
        copy.wait_send()
    for item in range(items):
        drain(item)


def shards(n, parts, tokens, w_query, w_key, w_value, cum_gate, w_out):
    deep, wide = dims(n)
    rows, width = tokens.shape
    block = rows * parts
    heads = cum_gate.shape[1]
    pc = w_key.shape[1]
    qc = w_query.shape[1]
    kw = pc if pc % LANES == 0 else 2 * pc
    cols = heads * block
    span = block * GATE_LANES // LANES
    local_kv = pc // HEAD_DIM
    pieces = chunk_count(parts)
    items = 2 + (parts - 1) * pieces
    dma = pltpu.SemaphoreType.DMA
    return pl.pallas_call(
        functools.partial(kernel, n, parts),
        out_shape=jax.ShapeDtypeStruct((rows, w_out.shape[1]), BF),
        in_specs=[pl.BlockSpec(memory_space=pltpu.HBM)] * 6,
        out_specs=pl.BlockSpec(memory_space=pltpu.VMEM),
        scratch_shapes=[
            pltpu.VMEM((parts, rows, width), BF),
            pltpu.VMEM(w_query.shape, BF),
            pltpu.VMEM((width, 2 * pc) if pc % LANES == 0 else (2, width, pc), BF),
            pltpu.VMEM(w_out.shape, BF),
            pltpu.VMEM((heads, block), F32),
            pltpu.VMEM((block, heads), F32),
            pltpu.VMEM((block, qc), BF),
            pltpu.VMEM((n, block, 2 * pc), BF),
            pltpu.VMEM((n, span, LANES), BF),
            pltpu.VMEM((n, block, LANES), BF),
            pltpu.VMEM((kw + LANES, cols), BF),
            pltpu.VMEM((1, cols), F32),
            pltpu.VMEM((1, cols), F32),
            pltpu.VMEM((HEAD_DIM, cols), F32),
            pltpu.VMEM((local_kv, parts, rows, qc // local_kv), BF),
            pltpu.VMEM((local_kv, parts, rows, qc // local_kv), BF),
            dma((6,)),
            dma((parts, pieces)),
            dma((parts, pieces)),
            dma((local_kv, parts)),
            dma((local_kv, parts)),
            dma((items, deep)),
            dma((items, deep, wide)),
            dma((items, deep, wide)),
            dma((items, n)),
        ],
        compiler_params=pltpu.CompilerParams(
            collective_id=0, has_side_effects=True, vmem_limit_bytes=VMEM_LIMIT
        ),
    )(tokens, w_query, w_key, w_value, cum_gate.T, w_out)


def solution(mesh):
    n, parts = mesh.shape["sp"], mesh.shape["tp"]
    placed = (
        P(("sp", "tp"), None),
        P(None, "tp"),
        P(None, "tp"),
        P(None, "tp"),
        P("sp", "tp"),
        P(),
    )
    return jax.shard_map(
        functools.partial(shards, n, parts),
        mesh=mesh,
        in_specs=placed,
        out_specs=P(("sp", "tp"), None),
        check_vma=False,
    )
```

time: 34.4 us -> 27.6 us (0.80)
  the two profiles are of different devices: /device:TPU:29 before, /device:TPU:24 now
where the time goes in v2:
time: 27.6 us; the launch traced here: 27.5 us
  Pallas kernels  25.8 us (93%)
  local copies, waits for them, and re-layouts  1.67 us (6%)
    pallas_call x1, Pallas kernels, shards(): pl.pallas_call(functools.partial(kernel, n, parts), out_shape=jax.ShapeDt...  25.8 us
    unnamed x1, local copies, waits for them, and re-layouts  1.67 us

profile of v2, /device:TPU:24, one launch (start us, length us, event | category | flops | bytes accessed | tf_op | source)
XLA Modules:
  0.0 27.5 jit_solution(16679028371738196982)
XLA Ops:
  0.0 25.8 %shard_map.64 = bf16[64,2048]{1,0:T(8,128)(2,1)} custom-call(bf16[64,2048]{1,0:T(8,128)(2,1)} %tok_hbm.1, bf16[2048,512]{1,0:T(8,128)(2,1)} %wq_hbm.1, bf16[2048,128]{1,0:T(8,128)(2,1)} %wk_hbm.1, bf16[2048,128]{1,0:T(8,128)(2,1)} %wv_hbm.1, f32[8,128]{1,0:T(8,128)} %bitcast.1, bf16[1024,2048]{1,0:T(8,128)(2,1)} %wo_hbm.1), custom_call_target="tpu_custom_call" | custom-call | tf_op jit(solution)/shard_map/pallas_call | solution.py:429
  25.8 1.7 %copy.8 = bf16[64,2048]{1,0:T(8,128)(2,1)} copy(bf16[64,2048]{1,0:T(8,128)(2,1)} %shard_map.64) | data formatting | bytes 524288
